TPU v7x, 32 devices: a whole 2x2x4 slice. The times are simulated.
32 devices in a mesh: sp: 16 (over z, y, core), tp: 2 (over x).
Axes of the slice: x: 2, y: 2, z: 4, core: 2. Of those that a mesh axis runs over, the one named last changes fastest.
Arguments:
- incoming_activity: bfloat16 [8192, 2048], P(('sp', 'tp')), may hold values from -6 to 6
- entry_standardize_factor: bfloat16 [2048], replicated, may hold values from 0.099609375 to 1.8984375
- recursive_entry_matrix: bfloat16 [2048, 2048], P(None, 'tp'), may hold values from -0.125 to 0.125
- final_switch_matrix: bfloat16 [2048, 2048], P(None, 'tp'), may hold values from -0.125 to 0.125
- averaging_entry_matrix: bfloat16 [2048, 1024], P(None, 'tp'), may hold values from -0.125 to 0.125
- percolumn_filter_coefficients: bfloat16 [4, 2048], P(None, 'tp'), may hold values from -3 to 3
- switch_tiled_matrices: bfloat16 [2, 2, 32, 64, 64], P(None, None, 'tp'), may hold values from -0.75 to 0.75
- prior_fading_odds: float32 [2, 2048], P(None, 'tp'), may hold values from 2.7 to 17
- speed_factors: float32 [2, 8192], P(None, 'sp'), may hold values from 0.4 to 2.5, as said below
- extra_fading_amounts: float32 [2, 8192], P(None, 'sp'), may hold values from -1.39 to 0, as said below
- averaging_cluster_matrices: bfloat16 [8, 128, 128], P('tp'), may hold values from -0.5 to 0.5
- averaging_feature_factor: bfloat16 [1024], P('tp'), may hold values from 0.099609375 to 1.8984375
- recursive_final_matrix: bfloat16 [2048, 2048], P('tp'), may hold values from -0.25 to 0.25
- averaging_final_matrix: bfloat16 [1024, 2048], P('tp'), may hold values from -0.1875 to 0.1875
Outputs:
- mixed: bfloat16 [8192, 2048], P(('sp', 'tp'))
Inputs may be any that keep to these rules, and one draw needn't show every extreme that they name: `speed_factors`: constant over each aligned block of 512 positions. `extra_fading_amounts`: each row has at most two nonzero entries.
All inputs are finite; a program needn't handle non-finite values.
Results may differ from a plain program's by a relative error of at most 0.017.
Values may be sent and summed in bfloat16 or wider, within the bound.
A program may use at most 128 MiB of HBM per device.

v0:
```python
import jax
import jax.numpy as jnp
from jax import lax
from jax.sharding import PartitionSpec as P

FADING_FACTOR = 8.0
epsilon = 1e-06
span_rows = 16


def padded(block, sides, width):
    for axis, dim in sides:
        count = lax.axis_size(axis)
        forward = [(i, i + 1) for i in range(count - 1)]
        backward = [(target, source) for source, target in forward]
        low = lax.ppermute(
            lax.slice_in_dim(block, block.shape[dim] - width, None, axis=dim), axis, forward
        )
        high = lax.ppermute(lax.slice_in_dim(block, 0, width, axis=dim), axis, backward)
        block = jnp.concatenate([low, block, high], axis=dim)
    return block


def combine(earlier, later):
    return (earlier[0] * later[0], later[0] * earlier[1] + later[1])


def product(left, right):
    return jnp.dot(left, right, preferred_element_type=jnp.float32)


def block_chain(log_keep, drive, backward):
    length, width = log_keep.shape
    count = length // span_rows
    logs = log_keep.reshape(count, span_rows, width)
    sources = drive.reshape(count, span_rows, width)
    running = jnp.cumsum(logs, axis=1)
    place = jnp.arange(span_rows, dtype=jnp.int32)
    if backward:
        running = running[:, -1:] - running + logs
        inside = place[None, :] >= place[:, None]
    else:
        inside = place[None, :] <= place[:, None]
    inside = inside[None, :, :, None]
    spread = running[:, :, None, :] - running[:, None, :, :]
    weights = jnp.where(inside, jnp.exp(jnp.where(inside, spread, 0.0)), 0.0)
    within = jnp.einsum("btsc,bsc->btc", weights, sources)
    decay = jnp.exp(running)
    ones = jnp.ones((1, width), jnp.float32)
    zeros = jnp.zeros((1, width), jnp.float32)
    if backward:
        ends = (decay[:, 0], within[:, 0])
        total_keep, total_state = lax.associative_scan(combine, ends, axis=0, reverse=True)
        prior_keep = jnp.concatenate([total_keep[1:], ones], axis=0)
        prior_state = jnp.concatenate([total_state[1:], zeros], axis=0)
    else:
        ends = (decay[:, -1], within[:, -1])
        total_keep, total_state = lax.associative_scan(combine, ends, axis=0)
        prior_keep = jnp.concatenate([ones, total_keep[:-1]], axis=0)
        prior_state = jnp.concatenate([zeros, total_state[:-1]], axis=0)
    keep_all = decay * prior_keep[:, None]
    local_all = within + decay * prior_state[:, None]
    return (keep_all.reshape(length, width), local_all.reshape(length, width))


def local(
    incoming_activity,
    entry_standardize_factor,
    recursive_entry_matrix,
    final_switch_matrix,
    averaging_entry_matrix,
    percolumn_filter_coefficients,
    switch_tiled_matrices,
    prior_fading_odds,
    speed_factors,
    extra_fading_amounts,
    averaging_cluster_matrices,
    averaging_feature_factor,
    recursive_final_matrix,
    averaging_final_matrix,
):
    state_width = recursive_entry_matrix.shape[1]
    pool_width = averaging_entry_matrix.shape[1]
    gain = entry_standardize_factor.astype(jnp.float32)
    values = lax.all_gather(incoming_activity, "tp", axis=0, tiled=True).astype(jnp.float32)
    scaled = values * lax.rsqrt(jnp.mean(values * values, axis=1, keepdims=True) + epsilon)
    normed = (scaled * gain).astype(jnp.bfloat16)
    projected = jnp.concatenate(
        [
            product(normed, weight).astype(jnp.bfloat16)
            for weight in (recursive_entry_matrix, final_switch_matrix, averaging_entry_matrix)
        ],
        axis=1,
    )
    length = projected.shape[0]
    state_input = projected[:, :state_width]
    gate_input = projected[:, state_width : 2 * state_width]
    pool_input = projected[:, 2 * state_width :]
    conv_rows = padded(state_input, (("sp", 0),), 2).astype(jnp.float32)
    filtered = percolumn_filter_coefficients[0].astype(jnp.float32) * conv_rows[0:length]
    for shift in range(1, percolumn_filter_coefficients.shape[0]):
        filtered = (
            filtered
            + percolumn_filter_coefficients[shift].astype(jnp.float32)
            * conv_rows[shift : shift + length]
        )
    filtered = filtered.astype(jnp.bfloat16)
    filtered_wide = filtered.astype(jnp.float32)
    blocks_here = switch_tiled_matrices.shape[2]
    block_width = switch_tiled_matrices.shape[3]
    gate_sums = jnp.einsum(
        "tbi,dqbij->tdqbj",
        filtered.reshape(length, blocks_here, block_width),
        switch_tiled_matrices,
        preferred_element_type=jnp.float32,
    ).reshape(length, 2, 2, state_width)
    remember_switch = jax.nn.sigmoid(gate_sums[:, :, 0])
    inlet = jax.nn.sigmoid(gate_sums[:, :, 1])
    fading_speed = jax.nn.softplus(-prior_fading_odds)
    logarithmic_persistence = (
        -FADING_FACTOR
        * jnp.transpose(speed_factors)[:, :, None]
        * remember_switch
        * fading_speed[None]
        + jnp.transpose(extra_fading_amounts)[:, :, None]
    )
    drive = jnp.sqrt(-jnp.expm1(2.0 * logarithmic_persistence)) * inlet * filtered_wide[:, None, :]
    forward_keep, forward_local = block_chain(logarithmic_persistence[:, 0], drive[:, 0], False)
    backward_keep, backward_local = block_chain(logarithmic_persistence[:, 1], drive[:, 1], True)
    zeros = jnp.zeros((state_width,), jnp.float32)
    summary = jnp.stack([forward_keep[-1], forward_local[-1], backward_keep[0], backward_local[0]])[
        None
    ]
    totals = lax.all_gather(summary, "sp", axis=0, tiled=True)
    place = lax.axis_index("sp")
    forward_all = lax.associative_scan(combine, (totals[:, 0], totals[:, 1]), axis=0)
    backward_all = lax.associative_scan(combine, (totals[:, 2], totals[:, 3]), axis=0, reverse=True)
    forward_before = jnp.concatenate([zeros[None], forward_all[1]], axis=0)
    backward_after = jnp.concatenate([backward_all[1], zeros[None]], axis=0)
    forward_carry = lax.dynamic_index_in_dim(forward_before, place, 0, keepdims=False)
    backward_carry = lax.dynamic_index_in_dim(backward_after, place + 1, 0, keepdims=False)
    state_sum = (
        forward_local
        + forward_keep * forward_carry[None]
        + backward_local
        + backward_keep * backward_carry[None]
    )
    state_mix = (jax.nn.gelu(gate_input.astype(jnp.float32)) * state_sum).astype(jnp.bfloat16)
    pool_rows = padded(pool_input, (("sp", 0),), 8).astype(jnp.float32)
    spans = []
    level = pool_rows
    for step in range(4):
        shift = 1 << step
        level = level[:-shift] + level[shift:]
        spans.append(level)
    group_width = averaging_cluster_matrices.shape[1]
    local_groups = pool_width // group_width
    group_index = (
        lax.axis_index("tp") * local_groups + jnp.arange(pool_width, dtype=jnp.int32) // group_width
    )
    window_code = group_index % 4
    position = lax.axis_index("sp") * length + jnp.arange(length, dtype=jnp.int32)
    total_length = length * lax.axis_size("sp")
    window_sum = jnp.zeros((length, pool_width), jnp.float32)
    counted = jnp.ones((length, pool_width), jnp.float32)
    for code in range(4):
        half = 1 << code
        begin = 8 - half
        chosen = (window_code == code)[None, :]
        window_count = (
            jnp.minimum(position + half, total_length) - jnp.maximum(position - half, 0)
        ).astype(jnp.float32)[:, None]
        window_sum = jnp.where(chosen, spans[code][begin : begin + length], window_sum)
        counted = jnp.where(chosen, window_count, counted)
    pooled = (window_sum / counted - pool_rows[8 : 8 + length]).astype(jnp.bfloat16)
    grouped = jnp.einsum(
        "tgi,gij->tgj",
        pooled.reshape(length, local_groups, group_width),
        averaging_cluster_matrices,
        preferred_element_type=jnp.float32,
    ).reshape(length, pool_width)
    pool_mix = (grouped * averaging_feature_factor.astype(jnp.float32)).astype(jnp.bfloat16)
    return lax.psum_scatter(
        (
            product(state_mix, recursive_final_matrix) + product(pool_mix, averaging_final_matrix)
        ).astype(jnp.bfloat16),
        "tp",
        scatter_dimension=0,
        tiled=True,
    )


def solution(mesh):
    in_specs = (
        P(("sp", "tp"), None),
        P(),
        P(None, "tp"),
        P(None, "tp"),
        P(None, "tp"),
        P(None, "tp"),
        P(None, None, "tp", None, None),
        P(None, "tp"),
        P(None, "sp"),
        P(None, "sp"),
        P("tp", None, None),
        P("tp"),
        P("tp", None),
        P("tp", None),
    )
    out_specs = P(("sp", "tp"), None)
    return jax.shard_map(local, mesh=mesh, in_specs=in_specs, out_specs=out_specs, check_vma=False)
```

profile of v0, /device:TPU:0, one launch (start us, length us, event | category | flops | bytes accessed | tf_op | source)
XLA Modules:
  0.0 251.2 jit_solution(8073936475268317214)
XLA Ops:
  6.6 0.7 all-gather.4.cloned.1.call-update
  7.3 0.7 convert_element_type.101
  8.0 0.7 convert_element_type.85
  8.7 1.6 copy.54
  10.5 34.2 %all-gather.4.cloned.1.call-done = bf16[512,2048]{1,0:T(8,128)(2,1)} async-done(((bf16[256,2048]{1,0:T(8,128)(2,1)}), bf16[512,2048]{1,0:T(8,128)(2,1)}) %all-gather.4.cloned.1.call-update) | async-done | bytes 2097168 | tf_op jit(solution)/shard_map/all_gather | solution.py:85
  44.7 2.2 fusion
  47.0 4.7 %convolution_convert_fusion = bf16[512,1024]{1,0:T(8,128)(2,1)S(1)} fusion(bf16[2048,1024]{1,0:T(8,128)(2,1)} %param.16, bf16[512,2048]{1,0:T(8,128)(2,1)S(1)} %copy-done.9, f32[2048]{0:T(1024)S(1)} %convert_element_type.85, f32[512]{0:T(512)S(1)} %add_rsqrt_fusion), kind=kOutput, calls=%fused_computation.44 | convolution fusion | flops 2152202240 | bytes 7350272 | tf_op jit(solution)/shard_map/dot_general | solution.py:29
  51.8 1.6 collective-permute-start
  53.3 1.3 collective-permute-start.1
  54.6 1.3 convolution_convert_fusion.2
  56.0 4.5 %collective-permute-start.2 = (bf16[8,512]{1,0:T(8,128)(2,1)S(1)}, bf16[8,512]{1,0:T(8,128)(2,1)S(1)}, u32[]{:S(2)}, u32[]{:S(2)}) collective-permute-start(bf16[8,512]{1,0:T(8,128)(2,1)S(1)} %get-tuple-element.24), channel_id=1, source_target_pairs={{0,2},{2,4},{4,6},{6,8},{8,10},{10,12},{12,14},{14,16},{16,18},{18... | collective-permute-start | bytes 24584 | tf_op jit(solution)/shard_map/ppermute | solution.py:16
  60.4 1.3 collective-permute-start.3
  61.8 0.3 maximum_convert_fusion
  62.1 2.6 %fusion.71 = (f32[512,1024]{1,0:T(8,128)}, bf16[512,1024]{1,0:T(8,128)(2,1)}) fusion(f32[516,1024]{1,0:T(8,128)S(1)} %maximum_convert_fusion, f32[1024]{0:T(1024)S(1)} %bitcast.154, f32[1024]{0:T(1024)S(1)} %bitcast.155, f32[1024]{0:T(1024)S(1)} %bitcast.153, f32[1024]{0:T(1024)S(1)} %bitcast.152), kind=kLoop, calls=%fused_computation.227 | loop fusion | flops 4718592 | bytes 11550720 | tf_op jit(solution)/shard_map/convert_element_type | solution.py:108
  64.7 2.8 %copy.53 = bf16[512,1024]{0,1:T(8,128)(2,1)} copy(bf16[512,1024]{1,0:T(8,128)(2,1)} %get-tuple-element.8) | data formatting | bytes 2097152 | tf_op jit(solution)/shard_map/convert_element_type | solution.py:107
  67.4 2.5 fusion.96
  69.9 1.8 copy.55
  71.7 4.2 %fusion.74 = (f32[512,2,1,1024]{0,3,2,1:T(8,128)}, f32[512,2,1,1024]{0,3,2,1:T(8,128)}) fusion(f32[512,2,2,1024]{0,3,2,1:T(8,128)S(1)} %bitcast.122), kind=kLoop, calls=%fused_computation.229 | loop fusion | bytes 16777216 | tf_op jit(solution)/shard_map/slice | solution.py:117
  75.9 5.4 %copy.92 = f32[512,2,1,1024]{3,0,1,2:T(8,128)} copy(f32[512,2,1,1024]{0,3,2,1:T(8,128)} %get-tuple-element.12) | data formatting | bytes 8388608
  81.3 5.4 %copy.93 = f32[512,2,1,1024]{3,0,1,2:T(8,128)} copy(f32[512,2,1,1024]{0,3,2,1:T(8,128)} %get-tuple-element.13) | data formatting | bytes 8388608
  86.7 7.3 %fusion.3 = (f32[512,2,1024]{2,0,1:T(8,128)S(1)}, f32[512,2,1024]{2,0,1:T(8,128)S(1)}) fusion(f32[512,2,1,1024]{3,0,1,2:T(8,128)} %copy.93, f32[512,1024]{1,0:T(8,128)} %get-tuple-element.7, f32[512,2]{0,1:T(2,128)S(1)} %bitcast.158, f32[2,1024]{1,0:T(2,128)S(1)} %compare_select_fusion, f32[512,2,1,1024]{3,0,1,2:T(8,128)} %copy.92, ...), kind=kLoop, calls=%fused_computation.8 | loop fusion | flops 13631488 | bytes 18890752 | tf_op jit(solution)/shard_map/mul | solution.py:127
  94.0 3.3 %fusion.75 = (f32[512,1,1024]{2,0,1:T(8,128)}, f32[512,1,1024]{2,0,1:T(8,128)S(1)}, f32[512,1,1024]{2,0,1:T(8,128)}, f32[512,1,1024]{2,0,1:T(8,128)}) fusion(f32[512,2,1024]{2,0,1:T(8,128)S(1)} %get-tuple-element.6, f32[512,2,1024]{2,0,1:T(8,128)S(1)} %get-tuple-element.5), kind=kLoop, calls=%fused_computation.230 | loop fusion | bytes 16777216 | tf_op jit(solution)/shard_map/slice | solution.py:128
  97.3 0.6 copy-done.1
  97.9 1.3 fusion.20
  99.2 3.6 %fusion.73 = (f32[32,16,1024]{2,0,1:T(8,128)S(1)}, f32[32,16,1024]{2,0,1:T(8,128)}, f32[32,16,1024]{2,0,1:T(8,128)}) fusion(f32[32,16,1024]{2,1,0:T(8,128)S(1)} %bitcast.124, f32[32,16,1024]{2,0,1:T(8,128)S(1)} %fusion.20, f32[32,1024]{1,0:T(8,128)S(1)} %slice_bitcast_fusion.2), kind=kLoop, calls=%fused_computation.228 | loop fusion | flops 1048576 | bytes 10616832 | tf_op jit(solution)/shard_map/exp | solution.py:48
  102.9 3.0 %copy.66 = f32[32,16,1024]{2,1,0:T(8,128)S(1)} copy(f32[32,16,1024]{2,0,1:T(8,128)} %get-tuple-element.10) | data formatting | bytes 4194304 | tf_op jit(solution)/shard_map/add | solution.py:40
  105.9 12.3 %multiply_reduce_fusion = f32[32,1024,16]{1,2,0:T(8,128)S(1)} fusion(f32[32,1024,16]{1,2,0:T(8,128)S(1)} %bitcast.139, f32[32,16,1024]{2,1,0:T(8,128)S(1)} %copy.66, pred[16,16]{1,0:T(8,128)(4,1)S(1)} %iota_compare_fusion), kind=kLoop, calls=%fused_computation | loop fusion | flops 41418752 | bytes 6291712
  118.2 1.2 copy.121
  119.6 0.2 slice.739
  119.8 0.2 slice.741
  119.9 0.2 slice.770
  120.1 0.2 slice.772
  120.9 4.3 %fusion.95 = (f32[32,16,1024]{2,0,1:T(8,128)S(1)}, f32[32,16,1024]{2,0,1:T(8,128)}) fusion(f32[32,16,1024]{2,1,0:T(8,128)} %bitcast.125), kind=kOutput, calls=%fused_computation.250 | output fusion | flops 7864320 | bytes 6291456 | tf_op jit(solution)/shard_map/jit(cumsum)/reduce_window_sum | solution.py:37
  125.3 3.0 %copy.59 = f32[32,16,1024]{2,1,0:T(8,128)S(1)} copy(f32[32,16,1024]{2,0,1:T(8,128)} %get-tuple-element.97) | data formatting | bytes 4194304 | tf_op jit(solution)/shard_map/jit(cumsum)/reduce_window_sum | solution.py:37
  128.3 12.1 %multiply_reduce_fusion.1 = f32[32,1024,16]{1,2,0:T(8,128)S(1)} fusion(f32[32,1024,16]{1,2,0:T(8,128)S(1)} %bitcast.138, f32[32,16,1024]{2,1,0:T(8,128)S(1)} %copy.59, pred[16,16]{1,0:T(8,128)(4,1)S(1)} %iota_compare_fusion.1), kind=kLoop, calls=%fused_computation.1 | loop fusion | flops 41418752 | bytes 6291712
  140.5 1.2 copy.122
  142.5 4.1 %copy.64 = f32[32,16,1024]{2,1,0:T(8,128)} copy(f32[32,16,1024]{2,0,1:T(8,128)} %get-tuple-element.11) | data formatting | bytes 4194304 | tf_op jit(solution)/shard_map/sub | solution.py:40
  146.6 0.2 slice.761
  146.8 0.2 slice.792
  147.8 0.5 slice.794
  148.2 3.7 %multiply_add_fusion = f32[32,16,1024]{2,0,1:T(8,128)S(1)} fusion(f32[32,1024]{1,0:T(8,128)S(1)} %concatenate.110, f32[32,1024,16]{1,2,0:T(8,128)} %copy-done.3, f32[32,16,1024]{2,0,1:T(8,128)} %get-tuple-element.10), kind=kLoop, calls=%fused_computation.39 | loop fusion | flops 1048576 | bytes 6422528 | tf_op jit(solution)/shard_map/add | solution.py:62
  152.0 1.2 copy.68
  153.2 1.4 copy-done.6
  154.6 0.2 slice.763
  154.9 2.8 %bitcast_multiply_fusion.2 = f32[512,1024]{1,0:T(8,128)S(1)} fusion(f32[32,16,1024]{2,1,0:T(8,128)} %copy.64, f32[32,1024]{1,0:T(8,128)S(1)} %concatenate.105, f32[512,2,1024]{2,0,1:T(8,128)} %copy-done.1), kind=kLoop, calls=%fused_computation.32 | loop fusion | flops 1048576 | bytes 6422528 | tf_op jit(solution)/shard_map/mul | solution.py:61
  157.7 1.4 copy-done.5
  159.9 3.7 %broadcast_multiply_fusion = (f32[32,16,1024]{2,0,1:T(8,128)S(1)}, f32[32,16,1024]{2,0,1:T(8,128)S(1)}) fusion(f32[32,1024]{1,0:T(8,128)S(1)} %concatenate.100, f32[32,16,1024]{2,0,1:T(8,128)} %get-tuple-element.97, f32[32,1024]{1,0:T(8,128)S(1)} %concatenate.95, f32[32,1024,16]{1,2,0:T(8,128)} %copy-done.4), kind=kLoop, calls=%fused_computation.62 | loop fusion | flops 1572864 | bytes 8650752 | tf_op jit(solution)/shard_map/mul | solution.py:61
  163.6 1.2 copy.62
  164.9 1.2 copy.61
  166.2 1.4 copy-done.8
  167.6 24.5 %all-gather.1 = f32[16,4,1024]{2,1,0:T(4,128)S(1)} all-gather(f32[1,4,1024]{2,1,0:T(4,128)S(1)} %maximum_bitcast_fusion), channel_id=2, replica_groups=mesh['sp'=16,'tp'=2] {'sp'}, dimensions={0}, use_global_device_ids=true | all-gather | bytes 278528 | tf_op jit(solution)/shard_map/all_gather | solution.py:134
  192.1 0.2 fusion.80
  193.1 0.4 slice.835
  193.8 0.2 slice.832
  194.6 0.2 slice.861
  194.8 0.2 slice.830
  195.3 0.2 rev.2
  195.6 13.8 %fusion.28 = f32[512,2048]{1,0:T(8,128)} fusion(bf16[1024,2048]{1,0:T(8,128)(2,1)} %param.26, f32[512,1024]{1,0:T(8,128)} %copy-done.5, f32[512,1024]{1,0:T(8,128)} %bitcast.133, f32[512,1024]{1,0:T(8,128)} %bitcast.137, f32[512,1024]{1,0:T(8,128)} %bitcast.135, bf16[2048,1024]{1,0:T(8,128)(2,1)} %param.17, f32[1024]{0:T(1024)S(1)} %bitcast.157, ...), kind=kOutput, calls=%fused_computation.63 | convolution fusion | flops 4308074496 | bytes 23087104 | tf_op jit(solution)/shard_map/dot_general | solution.py:29
  210.0 0.3 fusion.77
  210.3 0.6 copy-done.19
  210.9 1.3 fusion.29
  212.3 0.8 copy-done.2
  213.1 2.6 %add_convert_fusion = bf16[512,2048]{1,0:T(8,128)(2,1)} fusion(f32[512,2048]{1,0:T(8,128)S(1)} %copy-done.2, bf16[512,512]{0,1:T(8,128)(2,1)S(1)} %fusion.27, bf16[512,2048]{1,0:T(8,128)(2,1)S(1)} %copy-done), kind=kOutput, calls=%fused_computation.12 | convolution fusion | flops 1075838976 | bytes 8912896 | tf_op jit(solution)/shard_map/dot_general | solution.py:29
  215.7 28.4 %reduce-scatter.2.cloned.1.call-done = bf16[256,2048]{1,0:T(8,128)(2,1)} async-done(((bf16[512,2048]{1,0:T(8,128)(2,1)}), bf16[256,2048]{1,0:T(8,128)(2,1)}) %reduce-scatter.2.cloned.1.call-update) | async-done | bytes 1048592 | tf_op jit(solution)/shard_map/reduce_scatter | solution.py:183
  (297 shorter events, 5.5 us)
Async XLA Ops:
  6.5 205.8 %copy-start = (bf16[512,2048]{1,0:T(8,128)(2,1)S(1)}, bf16[512,2048]{1,0:T(8,128)(2,1)}, u32[]{:S(2)}) copy-start(bf16[512,2048]{1,0:T(8,128)(2,1)} %param.27) | copy-start | bytes 6291460
  6.5 3.9 %copy-start.16 = (f32[2,512]{1,0:T(2,128)S(1)}, f32[2,512]{1,0:T(2,128)}, u32[]{:S(2)}) copy-start(f32[2,512]{1,0:T(2,128)} %param.22) | copy-start | bytes 12292
  6.5 3.9 %copy-start.15 = (f32[2,1024]{1,0:T(2,128)S(1)}, f32[2,1024]{1,0:T(2,128)}, u32[]{:S(2)}) copy-start(f32[2,1024]{1,0:T(2,128)} %param.21) | copy-start | bytes 24580
  6.5 3.9 %copy-start.14 = (bf16[4,1024]{1,0:T(4,128)(2,1)S(1)}, bf16[4,1024]{1,0:T(4,128)(2,1)}, u32[]{:S(2)}) copy-start(bf16[4,1024]{1,0:T(4,128)(2,1)} %param.19) | copy-start | bytes 24580
  6.5 38.2 %all-gather.4.cloned.1.call-start = ((), (), s32[]{:S(2)}) async-start(), calls=%async_computation.1 | async-start | bytes 3145728 | tf_op jit(solution)/shard_map/all_gather | solution.py:85
  7.3 236.9 %reduce-scatter.2.cloned.1.call-start = ((), (), s32[]{:S(2)}) async-start(), calls=%async_computation.2 | async-start | bytes 3145728 | tf_op jit(solution)/shard_map/reduce_scatter | solution.py:183
  44.7 2.2 copy-start.9
  47.0 7.6 %copy-start.18 = (bf16[2048,512]{1,0:T(8,128)(2,1)S(1)}, bf16[2048,512]{1,0:T(8,128)(2,1)}, u32[]{:S(2)}) copy-start(bf16[2048,512]{1,0:T(8,128)(2,1)} %param.18) | copy-start | bytes 6291460
  51.8 10.0 %collective-permute-start = (bf16[2,1024]{1,0:T(2,128)(2,1)S(1)}, bf16[2,1024]{1,0:T(2,128)(2,1)S(1)}, u32[]{:S(2)}, u32[]{:S(2)}) collective-permute-start(bf16[2,1024]{1,0:T(2,128)(2,1)S(1)} %get-tuple-element.22), channel_id=1, source_target_pairs={{0,2},{2,4},{4,6},{6,8},{8,10},{10,12},{12,14},{14,16},{16,18},{18... | collective-permute-start | bytes 12296 | tf_op jit(solution)/shard_map/ppermute | solution.py:16
  53.3 8.4 %collective-permute-start.1 = (bf16[2,1024]{1,0:T(2,128)(2,1)S(1)}, bf16[2,1024]{1,0:T(2,128)(2,1)S(1)}, u32[]{:S(2)}, u32[]{:S(2)}) collective-permute-start(bf16[2,1024]{1,0:T(2,128)(2,1)S(1)} %get-tuple-element.23), channel_id=1, source_target_pairs={{2,0},{4,2},{6,4},{8,6},{10,8},{12,10},{14,12},{16,14},{18,16},{20... | collective-permute-start | bytes 12296 | tf_op jit(solution)/shard_map/ppermute | solution.py:19
  55.9 6.1 %copy-start.12 = (bf16[512,512]{1,0:T(8,128)(2,1)}, bf16[512,512]{1,0:T(8,128)(2,1)S(1)}, u32[]{:S(2)}) copy-start(bf16[512,512]{1,0:T(8,128)(2,1)S(1)} %convolution_convert_fusion.2) | copy-start | bytes 1572868
  56.0 153.4 %collective-permute-start.2 = (bf16[8,512]{1,0:T(8,128)(2,1)S(1)}, bf16[8,512]{1,0:T(8,128)(2,1)S(1)}, u32[]{:S(2)}, u32[]{:S(2)}) collective-permute-start(bf16[8,512]{1,0:T(8,128)(2,1)S(1)} %get-tuple-element.24), channel_id=1, source_target_pairs={{0,2},{2,4},{4,6},{6,8},{8,10},{10,12},{12,14},{14,16},{16,18},{18... | collective-permute-start | bytes 24584 | tf_op jit(solution)/shard_map/ppermute | solution.py:16
  60.4 148.9 %collective-permute-start.3 = (bf16[8,512]{1,0:T(8,128)(2,1)S(1)}, bf16[8,512]{1,0:T(8,128)(2,1)S(1)}, u32[]{:S(2)}, u32[]{:S(2)}) collective-permute-start(bf16[8,512]{1,0:T(8,128)(2,1)S(1)} %get-tuple-element.25), channel_id=1, source_target_pairs={{2,0},{4,2},{6,4},{8,6},{10,8},{12,10},{14,12},{16,14},{18,16},{20... | collective-permute-start | bytes 24584 | tf_op jit(solution)/shard_map/ppermute | solution.py:19
  81.3 5.4 %copy-start.17 = (f32[2,512]{1,0:T(2,128)S(1)}, f32[2,512]{1,0:T(2,128)}, u32[]{:S(2)}) copy-start(f32[2,512]{1,0:T(2,128)} %param.23) | copy-start | bytes 12292
  94.0 3.9 %copy-start.1 = (f32[512,2,1024]{2,0,1:T(8,128)}, f32[512,2,1024]{2,0,1:T(8,128)S(1)}, u32[]{:S(2)}) copy-start(f32[512,2,1024]{2,0,1:T(8,128)S(1)} %get-tuple-element.6) | copy-start | bytes 12582916
  102.9 3.0 %copy-start.11 = (f32[512,1,1024]{2,0,1:T(8,128)S(1)}, f32[512,1,1024]{2,0,1:T(8,128)}, u32[]{:S(2)}) copy-start(f32[512,1,1024]{2,0,1:T(8,128)} %get-tuple-element.98) | copy-start | bytes 6291460
  118.2 1.3 copy-start.3
  125.3 3.0 %copy-start.10 = (f32[512,1,1024]{2,0,1:T(8,128)S(1)}, f32[512,1,1024]{2,0,1:T(8,128)}, u32[]{:S(2)}) copy-start(f32[512,1,1024]{2,0,1:T(8,128)} %get-tuple-element.99) | copy-start | bytes 6291460
  140.4 1.3 copy-start.4
  153.2 1.4 copy-start.6
  157.7 1.4 copy-start.5
  164.9 1.3 copy-start.7
  166.2 1.4 copy-start.8
  195.6 13.8 %copy-start.13 = (bf16[512,512]{1,0:T(8,128)(2,1)S(1)}, bf16[512,512]{1,0:T(8,128)(2,1)}, u32[]{:S(2)}) copy-start(bf16[512,512]{1,0:T(8,128)(2,1)} %copy-done.12) | copy-start | bytes 1572868
  210.0 0.9 copy-start.19
  210.9 2.2 copy-start.2
Sparse Core Ops, SparseCore 0:
  8.9 35.8 all-gather.3
  215.9 28.2 reduce-scatter.1
where the time goes:
time: 256 us; the launch traced here: 251 us
  waiting for transfers between devices  63.3 us (25%)
  other arithmetic  59.5 us (23%)
  local copies, waits for them, and re-layouts  53.5 us (21%)
  matrix products  26.1 us (10%)
  blocking collectives  24.5 us (10%)
  between operations  15.5 us (6%)
  starting transfers between devices  8.69 us (3%)
    all_gather x1, waiting for transfers between devices, local(): lax.all_gather(incoming_activity, 'tp', axis=0, tiled=True)  34.2 us
    reduce_scatter x1, waiting for transfers between devices, local(): lax.psum_scatter((product(state_mix, recursive_final_matrix) + product(po...  28.4 us
    all_gather x1, blocking collectives, local(): totals = lax.all_gather(summary, 'sp', axis=0, tiled=True)  24.5 us
    unnamed x3, other arithmetic  24.5 us
    dot_general x4, matrix products, product(): return jnp.dot(left, right, preferred_element_type=jnp.float32)  22.4 us
    unnamed x51, local copies, waits for them, and re-layouts  18.9 us
    mul x1, other arithmetic, local(): jnp.sqrt(-jnp.expm1(2.0 * logarithmic_persistence)) * inlet  7.26 us
    mul x2, other arithmetic, block_chain(): keep_all = decay * prior_keep[:, None]  6.51 us
  transfers between devices with their start and end apart: 6, of which 2 were waited for; matrix products, arithmetic and copies ran while one was open for 48% of the time, Pallas kernels for 0%

commit v1 on v0

--- a/solution.py
+++ b/solution.py
@@ -1,3 +1,4 @@
+import functools
 import jax
 import jax.numpy as jnp
 from jax import lax
@@ -6,6 +7,31 @@
 FADING_FACTOR = 8.0
 epsilon = 1e-06
 span_rows = 16
+
+
+def assign_space(raw, row_axis, axis_no):
+    r2 = lax.axis_size(row_axis)
+    n_now, response, r1 = (r2, lax.axis_index(row_axis), raw.shape[axis_no])
+    stack_in = [(idx, (idx + 1) % n_now) for idx in range(n_now)]
+    heap = [(idx, (idx - 1) % n_now) for idx in range(n_now)]
+    y1 = jnp.zeros((*raw.shape[:axis_no], n_now * r1, *raw.shape[axis_no + 1 :]), raw.dtype)
+    y1 = lax.dynamic_update_slice_in_dim(y1, raw, response * r1, axis=axis_no)
+    mixed_arr = latest = raw
+    next_value = n_now // 2
+    for k0 in range(1, next_value + 1):
+        mixed_arr = lax.ppermute(mixed_arr, axis_name=row_axis, perm=stack_in)
+        y1 = lax.dynamic_update_slice_in_dim(
+            y1, mixed_arr, (response - k0) % n_now * r1, axis=axis_no
+        )
+        if k0 < n_now - next_value:
+            latest = lax.ppermute(latest, perm=heap, axis_name=row_axis)
+            y1 = lax.dynamic_update_slice_in_dim(
+                y1, latest, (response + k0) % n_now * r1, axis=axis_no
+            )
+    return y1
+
+
+refer_the_patches = functools.partial(assign_space, row_axis="sp", axis_no=0)
 
 
 def padded(block, sides, width):
@@ -131,7 +157,7 @@
     summary = jnp.stack([forward_keep[-1], forward_local[-1], backward_keep[0], backward_local[0]])[
         None
     ]
-    totals = lax.all_gather(summary, "sp", axis=0, tiled=True)
+    totals = refer_the_patches(summary)
     place = lax.axis_index("sp")
     forward_all = lax.associative_scan(combine, (totals[:, 0], totals[:, 1]), axis=0)
     backward_all = lax.associative_scan(combine, (totals[:, 2], totals[:, 3]), axis=0, reverse=True)

time: 256 us -> 278 us (1.086)
  starting transfers between devices: 8.69 us -> 39.7 us
  blocking collectives: 24.5 us -> 0 us
  waiting for transfers between devices: 63.3 us -> 75.3 us
  matrix products: 26.1 us -> 29.1 us
    ppermute x0 -> x15, starting transfers between devices: none -> 32.7 us  [the longest x7 30 us: assign_space(): latest = lax.ppermute(latest, perm=heap, axis_name=row_axis)]
    all_gather x1 -> x0, blocking collectives: 24.5 us -> none  [local(): totals = lax.all_gather(summary, 'sp', axis=0, tiled=True)]
    ppermute x0 -> x15, waiting for transfers between devices: none -> 9.6 us  [the longest x7 5.01 us: assign_space(): latest = lax.ppermute(latest, perm=heap, axis_name=row_axis)]
    dot_general x4, matrix products: 22.4 us -> 25.4 us  [product(): return jnp.dot(left, right, preferred_element_type=jnp.float32)]
    unnamed x51 -> x45, local copies, waits for them, and re-layouts: 18.9 us -> 17.4 us
    unnamed x3 -> x2, other arithmetic: 24.5 us -> 24.5 us
  transfers between devices with their start and end apart: 6 -> 21, of which waited for: 2 -> 15; matrix products, arithmetic and copies ran while one was open for 48% -> 3% of each run, Pallas kernels for 0% -> 0%
where the time goes in v1:
time: 278 us; the launch traced here: 273 us
  waiting for transfers between devices  75.3 us (27%)
  other arithmetic  58.9 us (21%)
  local copies, waits for them, and re-layouts  54.1 us (19%)
  starting transfers between devices  39.7 us (14%)
  matrix products  29.1 us (10%)
  between operations  16 us (6%)
    all_gather x1, waiting for transfers between devices, local(): lax.all_gather(incoming_activity, 'tp', axis=0, tiled=True)  34.8 us
    ppermute x7, starting transfers between devices, assign_space(): latest = lax.ppermute(latest, perm=heap, axis_name=row_axis)  30 us
    reduce_scatter x1, waiting for transfers between devices, local(): lax.psum_scatter((product(state_mix, recursive_final_matrix) + product(po...  29.2 us
    dot_general x4, matrix products, product(): return jnp.dot(left, right, preferred_element_type=jnp.float32)  25.4 us
    unnamed x2, other arithmetic  24.5 us
    unnamed x45, local copies, waits for them, and re-layouts  17.4 us
    mul x1, other arithmetic, local(): jnp.sqrt(-jnp.expm1(2.0 * logarithmic_persistence)) * inlet  7.26 us
    mul x2, other arithmetic, block_chain(): keep_all = decay * prior_keep[:, None]  6.51 us
  transfers between devices with their start and end apart: 21, of which 15 were waited for; matrix products, arithmetic and copies ran while one was open for 3% of the time, Pallas kernels for 0%

profile of v1, /device:TPU:0, one launch (start us, length us, event | category | flops | bytes accessed | tf_op | source)
XLA Modules:
  0.0 273.1 jit_solution(18295501291454773432)
XLA Ops:
  6.6 0.7 all-gather.2.cloned.1.call-update
  7.4 0.7 convert_element_type.85
  8.1 1.6 copy.52
  9.9 34.8 %all-gather.2.cloned.1.call-done = bf16[512,2048]{1,0:T(8,128)(2,1)} async-done(((bf16[256,2048]{1,0:T(8,128)(2,1)}), bf16[512,2048]{1,0:T(8,128)(2,1)}) %all-gather.2.cloned.1.call-update) | async-done | bytes 2097168 | tf_op jit(solution)/shard_map/all_gather | solution.py:111
  44.7 2.2 fusion
  47.0 4.7 %convolution_convert_fusion = bf16[512,1024]{1,0:T(8,128)(2,1)S(1)} fusion(bf16[2048,1024]{1,0:T(8,128)(2,1)} %param.16, bf16[512,2048]{1,0:T(8,128)(2,1)S(1)} %copy-done.8, f32[2048]{0:T(1024)S(1)} %convert_element_type.85, f32[512]{0:T(512)S(1)} %add_rsqrt_fusion), kind=kOutput, calls=%fused_computation.44 | convolution fusion | flops 2152202240 | bytes 7350272 | tf_op jit(solution)/shard_map/dot_general | solution.py:55
  51.7 1.6 collective-permute-start
  53.3 1.3 collective-permute-start.1
  54.6 2.1 convolution_convert_fusion.2
  56.7 1.1 collective-permute-done.1
  57.8 0.3 maximum_convert_fusion
  58.1 2.6 fusion.71
  60.7 2.4 copy.51
  63.1 2.4 fusion.95
  65.6 1.8 copy.53
  67.4 4.2 %fusion.74 = (f32[512,2,1,1024]{0,3,2,1:T(8,128)}, f32[512,2,1,1024]{0,3,2,1:T(8,128)}) fusion(f32[512,2,2,1024]{0,3,2,1:T(8,128)S(1)} %bitcast.124), kind=kLoop, calls=%fused_computation.229 | loop fusion | bytes 16777216 | tf_op jit(solution)/shard_map/slice | solution.py:143
  71.6 5.4 %copy.108 = f32[512,2,1,1024]{3,0,1,2:T(8,128)} copy(f32[512,2,1,1024]{0,3,2,1:T(8,128)} %get-tuple-element.12) | data formatting | bytes 8388608
  77.0 5.4 %copy.109 = f32[512,2,1,1024]{3,0,1,2:T(8,128)} copy(f32[512,2,1,1024]{0,3,2,1:T(8,128)} %get-tuple-element.13) | data formatting | bytes 8388608
  82.4 7.3 %fusion.3 = (f32[512,2,1024]{2,0,1:T(8,128)S(1)}, f32[512,2,1024]{2,0,1:T(8,128)S(1)}) fusion(f32[512,2,1,1024]{3,0,1,2:T(8,128)} %copy.109, f32[512,1024]{1,0:T(8,128)} %get-tuple-element.7, f32[512,2]{0,1:T(2,128)S(1)} %bitcast.148, f32[2,1024]{1,0:T(2,128)S(1)} %compare_select_fusion, f32[512,2,1,1024]{3,0,1,2:T(8,128)} %copy.108, ...), kind=kLoop, calls=%fused_computation.8 | loop fusion | flops 13631488 | bytes 18890752 | tf_op jit(solution)/shard_map/mul | solution.py:153
  89.7 3.3 %fusion.75 = (f32[512,1,1024]{2,0,1:T(8,128)}, f32[512,1,1024]{2,0,1:T(8,128)S(1)}, f32[512,1,1024]{2,0,1:T(8,128)}, f32[512,1,1024]{2,0,1:T(8,128)}) fusion(f32[512,2,1024]{2,0,1:T(8,128)S(1)} %get-tuple-element.6, f32[512,2,1024]{2,0,1:T(8,128)S(1)} %get-tuple-element.5), kind=kLoop, calls=%fused_computation.230 | loop fusion | bytes 16777216 | tf_op jit(solution)/shard_map/slice | solution.py:154
  92.9 0.6 copy-done.1
  93.6 1.3 fusion.20
  94.9 3.6 %fusion.73 = (f32[32,16,1024]{2,0,1:T(8,128)S(1)}, f32[32,16,1024]{2,0,1:T(8,128)}, f32[32,16,1024]{2,0,1:T(8,128)}) fusion(f32[32,16,1024]{2,1,0:T(8,128)S(1)} %bitcast.126, f32[32,16,1024]{2,0,1:T(8,128)S(1)} %fusion.20, f32[32,1024]{1,0:T(8,128)S(1)} %slice_bitcast_fusion.2), kind=kLoop, calls=%fused_computation.228 | loop fusion | flops 1048576 | bytes 10616832 | tf_op jit(solution)/shard_map/exp | solution.py:74
  98.6 3.0 %copy.64 = f32[32,16,1024]{2,1,0:T(8,128)S(1)} copy(f32[32,16,1024]{2,0,1:T(8,128)} %get-tuple-element.10) | data formatting | bytes 4194304 | tf_op jit(solution)/shard_map/add | solution.py:66
  101.6 12.3 %multiply_reduce_fusion = f32[32,1024,16]{1,2,0:T(8,128)S(1)} fusion(f32[32,1024,16]{1,2,0:T(8,128)S(1)} %bitcast.141, f32[32,16,1024]{2,1,0:T(8,128)S(1)} %copy.64, pred[16,16]{1,0:T(8,128)(4,1)S(1)} %iota_compare_fusion), kind=kLoop, calls=%fused_computation | loop fusion | flops 41418752 | bytes 6291712
  113.9 1.2 copy.135
  116.6 4.3 %fusion.94 = (f32[32,16,1024]{2,0,1:T(8,128)S(1)}, f32[32,16,1024]{2,0,1:T(8,128)}) fusion(f32[32,16,1024]{2,1,0:T(8,128)} %bitcast.127), kind=kOutput, calls=%fused_computation.249 | output fusion | flops 7864320 | bytes 6291456 | tf_op jit(solution)/shard_map/jit(cumsum)/reduce_window_sum | solution.py:63
  121.1 3.0 %copy.57 = f32[32,16,1024]{2,1,0:T(8,128)S(1)} copy(f32[32,16,1024]{2,0,1:T(8,128)} %get-tuple-element.97) | data formatting | bytes 4194304 | tf_op jit(solution)/shard_map/jit(cumsum)/reduce_window_sum | solution.py:63
  124.0 12.1 %multiply_reduce_fusion.1 = f32[32,1024,16]{1,2,0:T(8,128)S(1)} fusion(f32[32,1024,16]{1,2,0:T(8,128)S(1)} %bitcast.140, f32[32,16,1024]{2,1,0:T(8,128)S(1)} %copy.57, pred[16,16]{1,0:T(8,128)(4,1)S(1)} %iota_compare_fusion.1), kind=kLoop, calls=%fused_computation.1 | loop fusion | flops 41418752 | bytes 6291712
  136.2 1.2 copy.136
  138.2 4.1 %copy.62 = f32[32,16,1024]{2,1,0:T(8,128)} copy(f32[32,16,1024]{2,0,1:T(8,128)} %get-tuple-element.11) | data formatting | bytes 4194304 | tf_op jit(solution)/shard_map/sub | solution.py:66
  143.5 0.6 slice.794
  144.2 3.7 %multiply_add_fusion = f32[32,16,1024]{2,0,1:T(8,128)S(1)} fusion(f32[32,1024]{1,0:T(8,128)S(1)} %concatenate.110, f32[32,1024,16]{1,2,0:T(8,128)} %copy-done.2, f32[32,16,1024]{2,0,1:T(8,128)} %get-tuple-element.10), kind=kLoop, calls=%fused_computation.39 | loop fusion | flops 1048576 | bytes 6422528 | tf_op jit(solution)/shard_map/add | solution.py:88
  147.9 1.2 copy.66
  149.1 1.4 copy-done.5
  150.8 2.8 %bitcast_multiply_fusion.2 = f32[512,1024]{1,0:T(8,128)S(1)} fusion(f32[32,16,1024]{2,1,0:T(8,128)} %copy.62, f32[32,1024]{1,0:T(8,128)S(1)} %concatenate.105, f32[512,2,1024]{2,0,1:T(8,128)} %copy-done.1), kind=kLoop, calls=%fused_computation.32 | loop fusion | flops 1048576 | bytes 6422528 | tf_op jit(solution)/shard_map/mul | solution.py:87
  153.6 1.4 copy-done.4
  155.8 3.7 %broadcast_multiply_fusion = (f32[32,16,1024]{2,0,1:T(8,128)S(1)}, f32[32,16,1024]{2,0,1:T(8,128)S(1)}) fusion(f32[32,1024]{1,0:T(8,128)S(1)} %concatenate.100, f32[32,16,1024]{2,0,1:T(8,128)} %get-tuple-element.97, f32[32,1024]{1,0:T(8,128)S(1)} %concatenate.95, f32[32,1024,16]{1,2,0:T(8,128)} %copy-done.3), kind=kLoop, calls=%fused_computation.62 | loop fusion | flops 1572864 | bytes 8650752 | tf_op jit(solution)/shard_map/mul | solution.py:87
  159.5 1.2 copy.60
  160.8 1.2 copy.59
  162.1 1.4 copy-done.7
  163.5 2.4 collective-permute-start.2
  165.9 2.7 %collective-permute-start.17 = (bf16[8,512]{1,0:T(8,128)(2,1)S(1)}, bf16[8,512]{1,0:T(8,128)(2,1)S(1)}, u32[]{:S(2)}, u32[]{:S(2)}) collective-permute-start(bf16[8,512]{1,0:T(8,128)(2,1)S(1)} %get-tuple-element.24), channel_id=1, source_target_pairs={{0,2},{2,4},{4,6},{6,8},{8,10},{10,12},{12,14},{14,16},{16,18},{18... | collective-permute-start | bytes 24584 | tf_op jit(solution)/shard_map/ppermute | solution.py:42
  168.6 1.3 collective-permute-start.18
  170.2 3.5 %collective-permute-start.3 = (f32[1,4,1024]{2,1,0:T(4,128)S(1)}, f32[1,4,1024]{2,1,0:T(4,128)S(1)}, u32[]{:S(2)}, u32[]{:S(2)}) collective-permute-start(f32[1,4,1024]{2,1,0:T(4,128)S(1)} %maximum_bitcast_fusion), channel_id=1, source_target_pairs={{0,30},{2,0},{4,2},{6,4},{8,6},{10,8},{12,10},{14,12},{16,14},{18,... | collective-permute-start | bytes 49160 | tf_op jit(solution)/shard_map/ppermute | solution.py:27
  174.1 1.0 collective-permute-done.3
  175.1 4.4 %collective-permute-start.5 = (f32[1,4,1024]{2,1,0:T(4,128)S(1)}, f32[1,4,1024]{2,1,0:T(4,128)S(1)}, u32[]{:S(2)}, u32[]{:S(2)}) collective-permute-start(f32[1,4,1024]{2,1,0:T(4,128)S(1)} %collective-permute-done.3), channel_id=1, source_target_pairs={{0,30},{2,0},{4,2},{6,4},{8,6},{10,8},{12,10},{14,12},{16,14},{18,... | collective-permute-start | bytes 49160 | tf_op jit(solution)/shard_map/ppermute | solution.py:27
  180.0 1.0 collective-permute-done.5
  181.0 4.4 %collective-permute-start.7 = (f32[1,4,1024]{2,1,0:T(4,128)S(1)}, f32[1,4,1024]{2,1,0:T(4,128)S(1)}, u32[]{:S(2)}, u32[]{:S(2)}) collective-permute-start(f32[1,4,1024]{2,1,0:T(4,128)S(1)} %collective-permute-done.5), channel_id=1, source_target_pairs={{0,30},{2,0},{4,2},{6,4},{8,6},{10,8},{12,10},{14,12},{16,14},{18,... | collective-permute-start | bytes 49160 | tf_op jit(solution)/shard_map/ppermute | solution.py:27
  185.8 1.0 collective-permute-done.7
  186.9 4.4 %collective-permute-start.9 = (f32[1,4,1024]{2,1,0:T(4,128)S(1)}, f32[1,4,1024]{2,1,0:T(4,128)S(1)}, u32[]{:S(2)}, u32[]{:S(2)}) collective-permute-start(f32[1,4,1024]{2,1,0:T(4,128)S(1)} %collective-permute-done.7), channel_id=1, source_target_pairs={{0,30},{2,0},{4,2},{6,4},{8,6},{10,8},{12,10},{14,12},{16,14},{18,... | collective-permute-start | bytes 49160 | tf_op jit(solution)/shard_map/ppermute | solution.py:27
  191.7 1.0 collective-permute-done.9
  192.7 4.4 %collective-permute-start.11 = (f32[1,4,1024]{2,1,0:T(4,128)S(1)}, f32[1,4,1024]{2,1,0:T(4,128)S(1)}, u32[]{:S(2)}, u32[]{:S(2)}) collective-permute-start(f32[1,4,1024]{2,1,0:T(4,128)S(1)} %collective-permute-done.9), channel_id=1, source_target_pairs={{0,30},{2,0},{4,2},{6,4},{8,6},{10,8},{12,10},{14,12},{16,14},{18,... | collective-permute-start | bytes 49160 | tf_op jit(solution)/shard_map/ppermute | solution.py:27
  197.2 0.3 collective-permute-done.10
  197.4 0.3 fusion.77
  197.7 0.9 collective-permute-done.11
  198.6 4.4 %collective-permute-start.13 = (f32[1,4,1024]{2,1,0:T(4,128)S(1)}, f32[1,4,1024]{2,1,0:T(4,128)S(1)}, u32[]{:S(2)}, u32[]{:S(2)}) collective-permute-start(f32[1,4,1024]{2,1,0:T(4,128)S(1)} %collective-permute-done.11), channel_id=1, source_target_pairs={{0,30},{2,0},{4,2},{6,4},{8,6},{10,8},{12,10},{14,12},{16,14},{18,... | collective-permute-start | bytes 49160 | tf_op jit(solution)/shard_map/ppermute | solution.py:27
  203.0 0.3 collective-permute-done.12
  203.5 1.2 fusion.29
  204.7 4.5 %collective-permute-start.15 = (f32[1,4,1024]{2,1,0:T(4,128)S(1)}, f32[1,4,1024]{2,1,0:T(4,128)S(1)}, u32[]{:S(2)}, u32[]{:S(2)}) collective-permute-start(f32[1,4,1024]{2,1,0:T(4,128)S(1)} %collective-permute-done.13), channel_id=1, source_target_pairs={{0,30},{2,0},{4,2},{6,4},{8,6},{10,8},{12,10},{14,12},{16,14},{18,... | collective-permute-start | bytes 49160 | tf_op jit(solution)/shard_map/ppermute | solution.py:27
  212.0 3.2 %collective-permute-done.16 = f32[1,4,1024]{2,1,0:T(4,128)S(1)} collective-permute-done((f32[1,4,1024]{2,1,0:T(4,128)S(1)}, f32[1,4,1024]{2,1,0:T(4,128)S(1)}, u32[]{:S(2)}, u32[]{:S(2)}) %collective-permute-start.16) | collective-permute-done | bytes 16416 | tf_op jit(solution)/shard_map/ppermute | solution.py:22
  218.3 13.7 %fusion.28 = f32[512,2048]{1,0:T(8,128)} fusion(bf16[1024,2048]{1,0:T(8,128)(2,1)} %param.26, f32[512,1024]{1,0:T(8,128)} %copy-done.4, f32[512,1024]{1,0:T(8,128)} %bitcast.135, f32[512,1024]{1,0:T(8,128)} %bitcast.139, f32[512,1024]{1,0:T(8,128)} %bitcast.137, bf16[2048,1024]{1,0:T(8,128)(2,1)} %param.17, f32[1024]{0:T(1024)S(1)} %bitcast.147, ...), kind=kOutput, calls=%fused_computation.63 | convolution fusion | flops 4308074496 | bytes 23087104 | tf_op jit(solution)/shard_map/dot_general | solution.py:55
  232.0 4.8 %add_convert_fusion = bf16[512,2048]{1,0:T(8,128)(2,1)} fusion(f32[512,2048]{1,0:T(8,128)} %fusion.28, bf16[512,512]{0,1:T(8,128)(2,1)S(1)} %fusion.27, bf16[512,2048]{1,0:T(8,128)(2,1)S(1)} %copy-done), kind=kOutput, calls=%fused_computation.12 | convolution fusion | flops 1075838976 | bytes 8912896 | tf_op jit(solution)/shard_map/dot_general | solution.py:55
  236.9 29.2 %reduce-scatter.2.cloned.1.call-done = bf16[256,2048]{1,0:T(8,128)(2,1)} async-done(((bf16[512,2048]{1,0:T(8,128)(2,1)}), bf16[256,2048]{1,0:T(8,128)(2,1)}) %reduce-scatter.2.cloned.1.call-update) | async-done | bytes 1048592 | tf_op jit(solution)/shard_map/reduce_scatter | solution.py:209
  (353 shorter events, 11.3 us)
Async XLA Ops:
  6.5 225.5 %copy-start = (bf16[512,2048]{1,0:T(8,128)(2,1)S(1)}, bf16[512,2048]{1,0:T(8,128)(2,1)}, u32[]{:S(2)}) copy-start(bf16[512,2048]{1,0:T(8,128)(2,1)} %param.27) | copy-start | bytes 6291460
  6.5 3.3 %copy-start.14 = (f32[2,512]{1,0:T(2,128)S(1)}, f32[2,512]{1,0:T(2,128)}, u32[]{:S(2)}) copy-start(f32[2,512]{1,0:T(2,128)} %param.22) | copy-start | bytes 12292
  6.5 3.3 %copy-start.13 = (f32[2,1024]{1,0:T(2,128)S(1)}, f32[2,1024]{1,0:T(2,128)}, u32[]{:S(2)}) copy-start(f32[2,1024]{1,0:T(2,128)} %param.21) | copy-start | bytes 24580
  6.5 3.4 %copy-start.12 = (bf16[4,1024]{1,0:T(4,128)(2,1)S(1)}, bf16[4,1024]{1,0:T(4,128)(2,1)}, u32[]{:S(2)}) copy-start(bf16[4,1024]{1,0:T(4,128)(2,1)} %param.19) | copy-start | bytes 24580
  6.5 38.2 %all-gather.2.cloned.1.call-start = ((), (), s32[]{:S(2)}) async-start(), calls=%async_computation.1 | async-start | bytes 3145728 | tf_op jit(solution)/shard_map/all_gather | solution.py:111
  7.3 258.8 %reduce-scatter.2.cloned.1.call-start = ((), (), s32[]{:S(2)}) async-start(), calls=%async_computation.2 | async-start | bytes 3145728 | tf_op jit(solution)/shard_map/reduce_scatter | solution.py:209
  44.7 2.2 copy-start.8
  47.0 7.7 %copy-start.17 = (bf16[2048,512]{1,0:T(8,128)(2,1)S(1)}, bf16[2048,512]{1,0:T(8,128)(2,1)}, u32[]{:S(2)}) copy-start(bf16[2048,512]{1,0:T(8,128)(2,1)} %param.18) | copy-start | bytes 6291460
  51.7 5.0 %collective-permute-start = (bf16[2,1024]{1,0:T(2,128)(2,1)S(1)}, bf16[2,1024]{1,0:T(2,128)(2,1)S(1)}, u32[]{:S(2)}, u32[]{:S(2)}) collective-permute-start(bf16[2,1024]{1,0:T(2,128)(2,1)S(1)} %get-tuple-element.22), channel_id=1, source_target_pairs={{0,2},{2,4},{4,6},{6,8},{8,10},{10,12},{12,14},{14,16},{16,18},{18... | collective-permute-start | bytes 12296 | tf_op jit(solution)/shard_map/ppermute | solution.py:42
  53.3 4.5 %collective-permute-start.1 = (bf16[2,1024]{1,0:T(2,128)(2,1)S(1)}, bf16[2,1024]{1,0:T(2,128)(2,1)S(1)}, u32[]{:S(2)}, u32[]{:S(2)}) collective-permute-start(bf16[2,1024]{1,0:T(2,128)(2,1)S(1)} %get-tuple-element.23), channel_id=1, source_target_pairs={{2,0},{4,2},{6,4},{8,6},{10,8},{12,10},{14,12},{16,14},{18,16},{20... | collective-permute-start | bytes 12296 | tf_op jit(solution)/shard_map/ppermute | solution.py:45
  77.0 5.4 %copy-start.15 = (f32[2,512]{1,0:T(2,128)S(1)}, f32[2,512]{1,0:T(2,128)}, u32[]{:S(2)}) copy-start(f32[2,512]{1,0:T(2,128)} %param.23) | copy-start | bytes 12292
  89.6 3.9 %copy-start.1 = (f32[512,2,1024]{2,0,1:T(8,128)}, f32[512,2,1024]{2,0,1:T(8,128)S(1)}, u32[]{:S(2)}) copy-start(f32[512,2,1024]{2,0,1:T(8,128)S(1)} %get-tuple-element.6) | copy-start | bytes 12582916
  98.6 3.0 %copy-start.10 = (f32[512,1,1024]{2,0,1:T(8,128)S(1)}, f32[512,1,1024]{2,0,1:T(8,128)}, u32[]{:S(2)}) copy-start(f32[512,1,1024]{2,0,1:T(8,128)} %get-tuple-element.98) | copy-start | bytes 6291460
  113.9 1.3 copy-start.2
  121.1 3.0 %copy-start.9 = (f32[512,1,1024]{2,0,1:T(8,128)S(1)}, f32[512,1,1024]{2,0,1:T(8,128)}, u32[]{:S(2)}) copy-start(f32[512,1,1024]{2,0,1:T(8,128)} %get-tuple-element.99) | copy-start | bytes 6291460
  136.2 1.3 copy-start.3
  149.1 1.4 copy-start.5
  153.6 1.4 copy-start.4
  160.8 1.3 copy-start.6
  160.8 5.1 %copy-start.11 = (bf16[512,512]{1,0:T(8,128)(2,1)S(1)}, bf16[512,512]{1,0:T(8,128)(2,1)}, u32[]{:S(2)}) copy-start(bf16[512,512]{1,0:T(8,128)(2,1)} %convolution_convert_fusion.2) | copy-start | bytes 1572868
  160.8 9.3 %copy-start.16 = (bf16[512]{0:T(512)(128)(2,1)S(1)}, bf16[512]{0:T(512)(128)(2,1)}, u32[]{:S(2)}) copy-start(bf16[512]{0:T(512)(128)(2,1)} %param.25) | copy-start | bytes 3076
  162.1 1.4 copy-start.7
  163.5 10.4 %collective-permute-start.2 = (f32[1,4,1024]{2,1,0:T(4,128)S(1)}, f32[1,4,1024]{2,1,0:T(4,128)S(1)}, u32[]{:S(2)}, u32[]{:S(2)}) collective-permute-start(f32[1,4,1024]{2,1,0:T(4,128)S(1)} %maximum_bitcast_fusion), channel_id=1, source_target_pairs={{0,2},{2,4},{4,6},{6,8},{8,10},{10,12},{12,14},{14,16},{16,18},{18... | collective-permute-start | bytes 49160 | tf_op jit(solution)/shard_map/ppermute | solution.py:22
  165.9 8.1 %collective-permute-start.17 = (bf16[8,512]{1,0:T(8,128)(2,1)S(1)}, bf16[8,512]{1,0:T(8,128)(2,1)S(1)}, u32[]{:S(2)}, u32[]{:S(2)}) collective-permute-start(bf16[8,512]{1,0:T(8,128)(2,1)S(1)} %get-tuple-element.24), channel_id=1, source_target_pairs={{0,2},{2,4},{4,6},{6,8},{8,10},{10,12},{12,14},{14,16},{16,18},{18... | collective-permute-start | bytes 24584 | tf_op jit(solution)/shard_map/ppermute | solution.py:42
  168.6 5.3 %collective-permute-start.18 = (bf16[8,512]{1,0:T(8,128)(2,1)S(1)}, bf16[8,512]{1,0:T(8,128)(2,1)S(1)}, u32[]{:S(2)}, u32[]{:S(2)}) collective-permute-start(bf16[8,512]{1,0:T(8,128)(2,1)S(1)} %get-tuple-element.25), channel_id=1, source_target_pairs={{2,0},{4,2},{6,4},{8,6},{10,8},{12,10},{14,12},{16,14},{18,16},{20... | collective-permute-start | bytes 24584 | tf_op jit(solution)/shard_map/ppermute | solution.py:45
  170.2 4.9 %collective-permute-start.3 = (f32[1,4,1024]{2,1,0:T(4,128)S(1)}, f32[1,4,1024]{2,1,0:T(4,128)S(1)}, u32[]{:S(2)}, u32[]{:S(2)}) collective-permute-start(f32[1,4,1024]{2,1,0:T(4,128)S(1)} %maximum_bitcast_fusion), channel_id=1, source_target_pairs={{0,30},{2,0},{4,2},{6,4},{8,6},{10,8},{12,10},{14,12},{16,14},{18,... | collective-permute-start | bytes 49160 | tf_op jit(solution)/shard_map/ppermute | solution.py:27
  173.9 5.9 %collective-permute-start.4 = (f32[1,4,1024]{2,1,0:T(4,128)S(1)}, f32[1,4,1024]{2,1,0:T(4,128)S(1)}, u32[]{:S(2)}, u32[]{:S(2)}) collective-permute-start(f32[1,4,1024]{2,1,0:T(4,128)S(1)} %collective-permute-done.2), channel_id=1, source_target_pairs={{0,2},{2,4},{4,6},{6,8},{8,10},{10,12},{12,14},{14,16},{16,18},{18... | collective-permute-start | bytes 49160 | tf_op jit(solution)/shard_map/ppermute | solution.py:22
  175.1 5.9 %collective-permute-start.5 = (f32[1,4,1024]{2,1,0:T(4,128)S(1)}, f32[1,4,1024]{2,1,0:T(4,128)S(1)}, u32[]{:S(2)}, u32[]{:S(2)}) collective-permute-start(f32[1,4,1024]{2,1,0:T(4,128)S(1)} %collective-permute-done.3), channel_id=1, source_target_pairs={{0,30},{2,0},{4,2},{6,4},{8,6},{10,8},{12,10},{14,12},{16,14},{18,... | collective-permute-start | bytes 49160 | tf_op jit(solution)/shard_map/ppermute | solution.py:27
  179.8 5.9 %collective-permute-start.6 = (f32[1,4,1024]{2,1,0:T(4,128)S(1)}, f32[1,4,1024]{2,1,0:T(4,128)S(1)}, u32[]{:S(2)}, u32[]{:S(2)}) collective-permute-start(f32[1,4,1024]{2,1,0:T(4,128)S(1)} %collective-permute-done.4), channel_id=1, source_target_pairs={{0,2},{2,4},{4,6},{6,8},{8,10},{10,12},{12,14},{14,16},{16,18},{18... | collective-permute-start | bytes 49160 | tf_op jit(solution)/shard_map/ppermute | solution.py:22
  181.0 5.9 %collective-permute-start.7 = (f32[1,4,1024]{2,1,0:T(4,128)S(1)}, f32[1,4,1024]{2,1,0:T(4,128)S(1)}, u32[]{:S(2)}, u32[]{:S(2)}) collective-permute-start(f32[1,4,1024]{2,1,0:T(4,128)S(1)} %collective-permute-done.5), channel_id=1, source_target_pairs={{0,30},{2,0},{4,2},{6,4},{8,6},{10,8},{12,10},{14,12},{16,14},{18,... | collective-permute-start | bytes 49160 | tf_op jit(solution)/shard_map/ppermute | solution.py:27
  185.7 5.9 %collective-permute-start.8 = (f32[1,4,1024]{2,1,0:T(4,128)S(1)}, f32[1,4,1024]{2,1,0:T(4,128)S(1)}, u32[]{:S(2)}, u32[]{:S(2)}) collective-permute-start(f32[1,4,1024]{2,1,0:T(4,128)S(1)} %collective-permute-done.6), channel_id=1, source_target_pairs={{0,2},{2,4},{4,6},{6,8},{8,10},{10,12},{12,14},{14,16},{16,18},{18... | collective-permute-start | bytes 49160 | tf_op jit(solution)/shard_map/ppermute | solution.py:22
  186.9 5.9 %collective-permute-start.9 = (f32[1,4,1024]{2,1,0:T(4,128)S(1)}, f32[1,4,1024]{2,1,0:T(4,128)S(1)}, u32[]{:S(2)}, u32[]{:S(2)}) collective-permute-start(f32[1,4,1024]{2,1,0:T(4,128)S(1)} %collective-permute-done.7), channel_id=1, source_target_pairs={{0,30},{2,0},{4,2},{6,4},{8,6},{10,8},{12,10},{14,12},{16,14},{18,... | collective-permute-start | bytes 49160 | tf_op jit(solution)/shard_map/ppermute | solution.py:27
  191.6 5.9 %collective-permute-start.10 = (f32[1,4,1024]{2,1,0:T(4,128)S(1)}, f32[1,4,1024]{2,1,0:T(4,128)S(1)}, u32[]{:S(2)}, u32[]{:S(2)}) collective-permute-start(f32[1,4,1024]{2,1,0:T(4,128)S(1)} %collective-permute-done.8), channel_id=1, source_target_pairs={{0,2},{2,4},{4,6},{6,8},{8,10},{10,12},{12,14},{14,16},{16,18},{18... | collective-permute-start | bytes 49160 | tf_op jit(solution)/shard_map/ppermute | solution.py:22
  191.7 11.8 %copy-start.18 = (bf16[4,128,128]{2,1,0:T(8,128)(2,1)S(1)}, bf16[4,128,128]{2,1,0:T(8,128)(2,1)}, u32[]{:S(2)}) copy-start(bf16[4,128,128]{2,1,0:T(8,128)(2,1)} %param.24) | copy-start | bytes 393220
  192.7 5.9 %collective-permute-start.11 = (f32[1,4,1024]{2,1,0:T(4,128)S(1)}, f32[1,4,1024]{2,1,0:T(4,128)S(1)}, u32[]{:S(2)}, u32[]{:S(2)}) collective-permute-start(f32[1,4,1024]{2,1,0:T(4,128)S(1)} %collective-permute-done.9), channel_id=1, source_target_pairs={{0,30},{2,0},{4,2},{6,4},{8,6},{10,8},{12,10},{14,12},{16,14},{18,... | collective-permute-start | bytes 49160 | tf_op jit(solution)/shard_map/ppermute | solution.py:27
  197.4 5.9 %collective-permute-start.12 = (f32[1,4,1024]{2,1,0:T(4,128)S(1)}, f32[1,4,1024]{2,1,0:T(4,128)S(1)}, u32[]{:S(2)}, u32[]{:S(2)}) collective-permute-start(f32[1,4,1024]{2,1,0:T(4,128)S(1)} %collective-permute-done.10), channel_id=1, source_target_pairs={{0,2},{2,4},{4,6},{6,8},{8,10},{10,12},{12,14},{14,16},{16,18},{18... | collective-permute-start | bytes 49160 | tf_op jit(solution)/shard_map/ppermute | solution.py:22
  198.6 6.1 %collective-permute-start.13 = (f32[1,4,1024]{2,1,0:T(4,128)S(1)}, f32[1,4,1024]{2,1,0:T(4,128)S(1)}, u32[]{:S(2)}, u32[]{:S(2)}) collective-permute-start(f32[1,4,1024]{2,1,0:T(4,128)S(1)} %collective-permute-done.11), channel_id=1, source_target_pairs={{0,30},{2,0},{4,2},{6,4},{8,6},{10,8},{12,10},{14,12},{16,14},{18,... | collective-permute-start | bytes 49160 | tf_op jit(solution)/shard_map/ppermute | solution.py:27
  203.3 6.0 %collective-permute-start.14 = (f32[1,4,1024]{2,1,0:T(4,128)S(1)}, f32[1,4,1024]{2,1,0:T(4,128)S(1)}, u32[]{:S(2)}, u32[]{:S(2)}) collective-permute-start(f32[1,4,1024]{2,1,0:T(4,128)S(1)} %collective-permute-done.12), channel_id=1, source_target_pairs={{0,2},{2,4},{4,6},{6,8},{8,10},{10,12},{12,14},{14,16},{16,18},{18... | collective-permute-start | bytes 49160 | tf_op jit(solution)/shard_map/ppermute | solution.py:22
  204.7 7.1 %collective-permute-start.15 = (f32[1,4,1024]{2,1,0:T(4,128)S(1)}, f32[1,4,1024]{2,1,0:T(4,128)S(1)}, u32[]{:S(2)}, u32[]{:S(2)}) collective-permute-start(f32[1,4,1024]{2,1,0:T(4,128)S(1)} %collective-permute-done.13), channel_id=1, source_target_pairs={{0,30},{2,0},{4,2},{6,4},{8,6},{10,8},{12,10},{14,12},{16,14},{18,... | collective-permute-start | bytes 49160 | tf_op jit(solution)/shard_map/ppermute | solution.py:27
  209.3 5.9 %collective-permute-start.16 = (f32[1,4,1024]{2,1,0:T(4,128)S(1)}, f32[1,4,1024]{2,1,0:T(4,128)S(1)}, u32[]{:S(2)}, u32[]{:S(2)}) collective-permute-start(f32[1,4,1024]{2,1,0:T(4,128)S(1)} %collective-permute-done.14), channel_id=1, source_target_pairs={{0,2},{2,4},{4,6},{6,8},{8,10},{10,12},{12,14},{14,16},{16,18},{18... | collective-permute-start | bytes 49160 | tf_op jit(solution)/shard_map/ppermute | solution.py:22
Sparse Core Ops, SparseCore 0:
  8.9 35.8 all-gather.1
  237.0 28.9 reduce-scatter.1
